TPU v7x, 32 devices: a whole 2x2x4 slice. The times are simulated.
32 devices in a mesh: sp: 8 (over z, y), tp: 4 (over x, core).
Axes of the slice: x: 2, y: 2, z: 4, core: 2. Of those that a mesh axis runs over, the one named last changes fastest.
Arguments:
- queries: bfloat16 [8192, 1024], P('sp', 'tp'), may hold values from -6 to 6
- keys: bfloat16 [8192, 1024], P('sp', 'tp'), may hold values from -6 to 6
- values: bfloat16 [8192, 1024], P('sp', 'tp'), may hold values from -6 to 6
- gates: bfloat16 [8192, 1024], P('sp', 'tp'), may hold values from -6 to 6
- log_decay: float32 [8192, 8], P('sp', 'tp'), may hold values from -1.6 to 0, as said below
- norm_gain: float32 [8, 128], P('tp'), may hold values from 0.1 to 1.9
- out_weight: bfloat16 [1024, 2048], P('tp'), may hold values from -0.1875 to 0.1875
- resid: bfloat16 [8192, 2048], P(('sp', 'tp')), may hold values from -6 to 6
- post_mix_gain: float32 [2048], replicated, may hold values from 0.1 to 1.9
- pre_ffn_gain: float32 [2048], replicated, may hold values from 0.1 to 1.9
- w_gate: bfloat16 [2048, 5632], P('sp', 'tp'), may hold values from -0.125 to 0.125
- w_up: bfloat16 [2048, 5632], P('sp', 'tp'), may hold values from -0.125 to 0.125
- w_down: bfloat16 [5632, 2048], P('tp', 'sp'), may hold values from -0.078125 to 0.078125
- post_ffn_gain: float32 [2048], replicated, may hold values from 0.1 to 1.9
Outputs:
- updated: bfloat16 [8192, 2048], P(('sp', 'tp'))
Inputs may be any that keep to these rules, and one draw needn't show every extreme that they name: `log_decay`: every entry is negative.
All inputs are finite; a program needn't handle non-finite values.
Results may differ from a plain program's by a relative error of at most 0.02.
Values may be sent and summed in bfloat16 or wider, within the bound.
A program may use at most 128 MiB of HBM per device.

v0:
```python
import jax
import jax.numpy as jnp
from jax import lax
from jax.experimental import pallas as pl
from jax.experimental.pallas import tpu as pltpu
from jax.sharding import PartitionSpec as P


BLOCK = 512


EPSILON = 1e-06
LONGEST_RING = 8


def entering(decay, state):
    place = lax.axis_index("sp")
    head_count, head_dim, _ = state.shape
    decay_rows = jnp.broadcast_to(decay[:, None, None], (head_count, 16, head_dim))
    packed = jnp.concatenate([state, decay_rows], axis=1).astype(jnp.bfloat16)
    gathered = lax.all_gather(packed, "sp")

    def one(step, running):
        piece = lax.dynamic_index_in_dim(gathered, step, 0, False).astype(jnp.float32)
        return piece[:, head_dim : head_dim + 1, :] * running + piece[:, :head_dim]

    return lax.fori_loop(0, place, one, jnp.zeros_like(state))


def from_earlier(packed, distance):
    count = lax.axis_size("sp")
    return lax.ppermute(packed, "sp", [(i, i + distance) for i in range(count - distance)])


def entering_by_hops(decay, state):
    count = lax.axis_size("sp")
    head_count, head_dim, _ = state.shape
    decay_rows = jnp.broadcast_to(decay[:, None, None], (head_count, 8, head_dim))
    packed = jnp.concatenate([state, decay_rows], axis=1)
    near = from_earlier(packed, 1)
    far = from_earlier(packed, 2)
    factor = near[:, head_dim:]
    pair = jnp.concatenate(
        [factor[:, :1] * far[:, :head_dim] + near[:, :head_dim], factor * far[:, head_dim:]],
        axis=1,
    )
    total, factor = pair[:, :head_dim], pair[:, head_dim : head_dim + 1]
    for piece in [from_earlier(pair, distance) for distance in range(2, count, 2)]:
        total = total + factor * piece[:, :head_dim]
        factor = factor * piece[:, head_dim : head_dim + 1]
    return total


def ring_order(count):
    return list(range(0, count, 2)) + list(range(1, count, 2))[::-1]


def ring_gather(block, forward_steps, backward_steps):
    count = lax.axis_size("sp")
    order = ring_order(count)
    ahead = [(order[i], order[(i + 1) % count]) for i in range(count)]
    behind = [(b, a) for a, b in ahead]
    arrived = [(0, block)]
    up, down = block, block
    for step in range(1, max(forward_steps, backward_steps) + 1):
        if step <= forward_steps:
            up = lax.ppermute(up, "sp", ahead)
            arrived.append((-step, up))
        if step <= backward_steps:
            down = lax.ppermute(down, "sp", behind)
            arrived.append((step, down))
    return arrived


def owner_of(offset):
    count = lax.axis_size("sp")
    me = lax.axis_index("sp")
    half = (count + 1) // 2
    position = jnp.where(me % 2 == 0, me // 2, count - 1 - me // 2)
    there = (position + offset + count) % count
    return jnp.where(there < half, 2 * there, 2 * (count - 1 - there) + 1)


def rms_norm(values_in, gain_vec):
    widened = values_in.astype(jnp.float32)
    return (
        widened
        * lax.rsqrt(jnp.mean(widened * widened, axis=-1, keepdims=True) + EPSILON)
        * gain_vec
    )


def block_step(carried, pieces):
    query_blk, key_blk, value_blk, decay_blk = pieces
    length = query_blk.shape[1]
    key_scale = query_blk.shape[2] ** (-0.5)
    cumulative = jnp.cumsum(decay_blk, axis=1)
    log_gap = cumulative[:, :, None] - cumulative[:, None, :]
    causal = lax.broadcasted_iota(jnp.int32, (length, length), 0) >= lax.broadcasted_iota(
        jnp.int32, (length, length), 1
    )
    weight = jnp.where(causal[None], jnp.exp(jnp.minimum(log_gap, 0.0)), 0.0)
    products = jnp.einsum("htd,hsd->hts", query_blk, key_blk, preferred_element_type=jnp.float32)
    scores = (products * key_scale * weight).astype(jnp.bfloat16)
    within = jnp.einsum("hts,hsd->htd", scores, value_blk, preferred_element_type=jnp.float32)
    carried_term = (
        jnp.einsum(
            "htd,hde->hte", query_blk.astype(jnp.float32), carried, precision=lax.Precision.HIGHEST
        )
        * jnp.exp(cumulative)[:, :, None]
    )
    to_end = jnp.exp(cumulative[:, -1:] - cumulative) * key_scale
    scaled_keys = (key_blk.astype(jnp.float32) * to_end[:, :, None]).astype(jnp.bfloat16)
    added = jnp.einsum("hsd,hse->hde", scaled_keys, value_blk, preferred_element_type=jnp.float32)
    carried = jnp.exp(cumulative[:, -1])[:, None, None] * carried + added
    return (carried, within + carried_term)


def to_blocks(matrix, block_len, head_count):
    row_count = matrix.shape[0]
    return matrix.reshape(row_count // block_len, block_len, head_count, -1).transpose(0, 2, 1, 3)


def finish_heads(retention, gates, norm_gain):
    centered = retention - jnp.mean(retention, axis=-1, keepdims=True)
    variance = jnp.mean(centered * centered, axis=-1, keepdims=True)
    normed = centered * lax.rsqrt(variance + EPSILON) * norm_gain[None]
    gate_vals = gates.astype(jnp.float32).reshape(normed.shape)
    return (jax.nn.silu(gate_vals) * normed).reshape(normed.shape[0], -1).astype(jnp.bfloat16)


def share_sum(part, row_count):
    count = lax.axis_size("tp")
    if count != 4:
        return lax.psum_scatter(part, "tp", scatter_dimension=0, tiled=True)
    me = lax.axis_index("tp")
    high, low = me // 2, me % 2
    shares = part.reshape(2, 2, row_count, -1)

    def swap(block, bit):
        return lax.ppermute(block, "tp", [(i, i ^ bit) for i in range(count)])

    def pick(block, index, dim):
        return lax.dynamic_index_in_dim(block, index, dim, False)

    nearer = swap(pick(shares, 1 - low, 1), 1).astype(jnp.float32)
    pair = pick(shares, low, 1).astype(jnp.float32) + nearer
    farther = swap(pick(pair, 1 - high, 0).astype(jnp.bfloat16), 2).astype(jnp.float32)
    return (pick(pair, high, 0) + farther).astype(jnp.bfloat16)


def ring_feed_forward(rows, gate_blocks, up_blocks, down_blocks, shape):
    depth = gate_blocks[0][1].shape[0]
    width = down_blocks[0][1].shape[1]
    half = (len(gate_blocks) + 1) // 2

    def project(blocks):
        total = None
        for some in (blocks[:half], blocks[half:]):
            if not some:
                continue
            columns = jnp.concatenate(
                [
                    lax.dynamic_slice_in_dim(rows, owner_of(offset) * depth, depth, 1)
                    for offset, _ in some
                ],
                axis=1,
            )
            weight = jnp.concatenate([block for _, block in some], axis=0)
            part = jnp.dot(columns, weight, preferred_element_type=jnp.float32)
            total = part if total is None else total + part
        return total

    gate_act = project(gate_blocks)
    up_act = project(up_blocks)
    hidden = (jax.nn.silu(gate_act) * up_act).astype(jnp.bfloat16)
    branch = jnp.zeros(shape, jnp.bfloat16)
    for some in (down_blocks[:half], down_blocks[half:]):
        if not some:
            continue
        wide = jnp.concatenate([block for _, block in some], axis=1)
        part = jnp.dot(hidden, wide, preferred_element_type=jnp.float32).astype(jnp.bfloat16)
        piece = share_sum(part, shape[0])
        for slot, (offset, _) in enumerate(some):
            branch = lax.dynamic_update_slice_in_dim(
                branch, piece[:, slot * width : (slot + 1) * width], owner_of(offset) * width, 1
            )
    return branch


def per_device(
    queries,
    keys,
    values,
    gates,
    log_decay,
    norm_gain,
    out_weight,
    resid,
    post_mix_gain,
    pre_ffn_gain,
    w_gate,
    w_up,
    w_down,
    post_ffn_gain,
):
    ring = lax.axis_size("sp")
    fewer = (ring - 1) // 2
    more = ring - 1 - fewer
    short = ring <= LONGEST_RING
    if short:
        gate_blocks = ring_gather(w_gate, more, fewer)
        up_blocks = ring_gather(w_up, fewer, more)
        down_blocks = ring_gather(w_down, more, fewer)
    row_count = queries.shape[0]
    head_count = log_decay.shape[1]
    head_dim = queries.shape[1] // head_count
    block_count = row_count // BLOCK
    query_blocks = to_blocks(queries, BLOCK, head_count)
    key_blocks = to_blocks(keys, BLOCK, head_count)
    value_blocks = to_blocks(values, BLOCK, head_count)
    decay_blocks = log_decay.reshape(block_count, BLOCK, head_count).transpose(0, 2, 1)
    start_state = jnp.zeros((head_count, head_dim, head_dim), jnp.float32)
    local_state, outputs = lax.scan(
        block_step, start_state, (query_blocks, key_blocks, value_blocks, decay_blocks)
    )
    retention = outputs.transpose(0, 2, 1, 3).reshape(row_count, head_count, head_dim)
    cumulative = jnp.cumsum(log_decay, axis=0)
    local_decay = jnp.exp(cumulative[-1])
    incoming = (entering_by_hops if short else entering)(local_decay, local_state)
    query_rows = queries.reshape(row_count, head_count, head_dim).astype(jnp.float32)
    retention = (
        retention
        + jnp.einsum("thd,hde->the", query_rows, incoming, precision=lax.Precision.HIGHEST)
        * jnp.exp(cumulative)[:, :, None]
    )
    retained = finish_heads(retention, gates, norm_gain)
    quarter = resid.shape[0]
    regrouped = lax.all_to_all(retained, "tp", split_axis=0, concat_axis=1, tiled=True)
    group_rows = out_weight.shape[0]
    empty_mix = jnp.zeros((quarter, out_weight.shape[1]), jnp.float32)
    running = empty_mix
    shard_piece = lax.all_gather(out_weight, "tp", axis=0, tiled=True)
    for offset in range(shard_piece.shape[0] // group_rows):
        columns = lax.dynamic_slice_in_dim(regrouped, offset * group_rows, group_rows, 1)
        part = jnp.dot(
            columns,
            shard_piece[offset * group_rows : (offset + 1) * group_rows],
            preferred_element_type=jnp.float32,
        )
        running = running + part.astype(jnp.bfloat16).astype(jnp.float32)
    mixed = running
    mixed = mixed.astype(jnp.bfloat16)
    middle = (resid.astype(jnp.float32) + rms_norm(mixed, post_mix_gain)).astype(jnp.bfloat16)
    ffn_input = rms_norm(middle, pre_ffn_gain).astype(jnp.bfloat16)
    gathered = lax.all_gather(ffn_input, "tp", axis=0, tiled=True)
    if not short:
        gate_act = jnp.dot(
            gathered,
            lax.all_gather(w_gate, "sp", axis=0, tiled=True),
            preferred_element_type=jnp.float32,
        )
        up_act = jnp.dot(
            gathered,
            lax.all_gather(w_up, "sp", axis=0, tiled=True),
            preferred_element_type=jnp.float32,
        )
        hidden = (jax.nn.silu(gate_act) * up_act).astype(jnp.bfloat16)
        down_full = lax.all_gather(w_down, "sp", axis=1, tiled=True)
        partial = jnp.dot(hidden, down_full, preferred_element_type=jnp.float32)
        branch = lax.psum_scatter(
            partial.astype(jnp.bfloat16), "tp", scatter_dimension=0, tiled=True
        )
    else:
        branch = ring_feed_forward(gathered, gate_blocks, up_blocks, down_blocks, resid.shape)
    return (middle.astype(jnp.float32) + rms_norm(branch, post_ffn_gain)).astype(jnp.bfloat16)


MESH = pl.DeviceIdType.MESH
HEADER_ROWS = 16
F32 = jnp.float32
BF16 = jnp.bfloat16


def silu_of(v):
    return v / (1.0 + jnp.exp(-v))


def layer_kernel(
    q_in,
    k_in,
    v_in,
    gates_in,
    decay_in,
    norm_gain,
    ow_in,
    resid_in,
    mix_gain,
    pre_gain,
    wg_in,
    wu_in,
    wd_in,
    post_gain,
    out,
    q_ref,
    k_ref,
    v_ref,
    gates_ref,
    resid_ref,
    wg,
    wu,
    wd,
    ow,
    cum_row,
    cum_col,
    local_state,
    start_state,
    state_out,
    state_pair,
    total_out,
    total_in,
    retention,
    retained_out,
    retained_in,
    mixed,
    middle,
    rows,
    hidden,
    part_out,
    part_in,
    sum_out,
    sum_in,
    branch,
    local_sem,
    own_sem,
    z_send,
    z_recv,
    y_send,
    y_recv,
    c_send,
    c_recv,
    ow_send,
    ow_recv,
    pair_send,
    pair_recv,
    total_send,
    total_recv,
    ret_send,
    ret_recv,
    rows_send,
    rows_recv,
    part_send,
    part_recv,
    sum_send,
    sum_recv,
):
    sp, tp = lax.axis_index("sp"), lax.axis_index("tp")
    planes = lax.axis_size("sp") // 2
    z, y = sp // 2, sp % 2
    x, core = tp // 2, tp % 2
    parity = z % 2
    pair = z + 1 - 2 * parity
    far = (z + 2) % planes
    far_pair = (pair + 2) % planes
    other_x, other_y, other_core = 1 - x, 1 - y, 1 - core
    is_main = core == parity
    is_helper = core != parity
    sp_y = z * 2 + other_y
    sp_pair = pair * 2 + y
    tp_x = other_x * 2 + core
    tp_core = x * 2 + other_core
    tp_both = other_x * 2 + other_core

    row_count, _ = q_ref.shape
    heads = norm_gain.shape[0]
    dim = norm_gain.shape[1]
    block_count = row_count // BLOCK
    quarter = resid_in.shape[0]
    model = resid_in.shape[1]
    units = wg_in.shape[1]
    tps = ow.shape[0]
    scale = dim ** (-0.5)

    inputs = [
        (k_in, k_ref),
        (v_in, v_ref),
        (q_in, q_ref),
        (gates_in, gates_ref),
        (resid_in, resid_ref),
        (ow_in, ow.at[tp]),
    ]

    def local_copy(i):
        return pltpu.make_async_copy(inputs[i][0], inputs[i][1], local_sem.at[i])

    weights_in = (wg_in, wu_in, wd_in)
    weights = (wg, wu, wd)

    def own_copy(m):
        return pltpu.make_async_copy(weights_in[m], weights[m].at[sp], own_sem.at[m])

    for i in range(len(inputs)):
        local_copy(i).start()

    @pl.when(is_main)
    def _():
        for m in range(3):
            own_copy(m).start()

    def remote(src, dst, send, recv, device):
        return pltpu.make_async_remote_copy(
            src_ref=src,
            dst_ref=dst,
            send_sem=send,
            recv_sem=recv,
            device_id=device,
            device_id_type=MESH,
        )

    barrier = pltpu.get_barrier_semaphore()
    peers = [(((z + i) % planes) * 2 + y, tp) for i in range(1, 4)]
    peers += [(sp_y, tp), (sp, tp_x), (sp, tp_core), (sp, tp_both), (sp_pair, tp_x)]
    for peer in peers:
        pl.semaphore_signal(barrier, inc=1, device_id=peer, device_id_type=MESH)
    pl.semaphore_wait(barrier, len(peers))

    far_target = lax.select(is_main, far, far_pair)

    def z_near(m):
        return remote(
            weights_in[m], weights[m].at[sp], z_send.at[m, 0], z_recv.at[m, z], (pair * 2 + y, tp)
        )

    def z_far(m):
        return remote(
            weights_in[m],
            weights[m].at[sp],
            z_send.at[m, 1],
            z_recv.at[m, z],
            (far_target * 2 + y, tp),
        )

    def start_z(m):
        @pl.when(is_helper)
        def _():
            z_near(m).start()

        z_far(m).start()

    def slot(m, source):
        return weights[m].at[source]

    def to_y(m, plane, src):
        place = plane * 2 + y
        return remote(
            src, slot(m, place), y_send.at[m, plane], y_recv.at[m, plane], (sp_y, tp)
        )

    def to_core(m, place, src):
        return remote(
            src, slot(m, place), c_send.at[m, place], c_recv.at[m, place], (sp, tp_core)
        )

    def z_arrival(m, plane):
        place = plane * 2 + y
        return remote(
            slot(m, place), slot(m, place), z_send.at[m, 1], z_recv.at[m, plane], (sp_y, tp)
        )

    def y_arrival(m, plane):
        place = plane * 2 + other_y
        return remote(
            slot(m, place), slot(m, place), y_send.at[m, plane], y_recv.at[m, plane], (sp_y, tp)
        )

    def start_own(m):
        @pl.when(is_main)
        def _():
            to_y(m, z, weights_in[m]).start()
            to_core(m, sp, weights_in[m]).start()

    def pass_z(m, planes_list):
        @pl.when(is_main)
        def _():
            for plane in planes_list:
                z_arrival(m, plane).wait_recv()
                place = plane * 2 + y
                to_y(m, plane, slot(m, place)).start()
                to_core(m, place, slot(m, place)).start()

    def pass_y(m, planes_list):
        @pl.when(is_main)
        def _():
            for plane in planes_list:
                y_arrival(m, plane).wait_recv()
                place = plane * 2 + other_y
                to_core(m, place, slot(m, place)).start()

    def core_wait(m, planes_list):
        @pl.when(is_helper)
        def _():
            for plane in planes_list:
                for place in (plane * 2 + y, plane * 2 + other_y):
                    to_core(m, place, slot(m, place)).wait_recv()

    def own_wait(m):
        @pl.when(is_main)
        def _():
            own_copy(m).wait()

    start_z(0)
    near_planes = [pair, far, far_pair]
    all_planes = [z] + near_planes

    ow_copies = [
        remote(ow_in, ow.at[tp], ow_send.at[0], ow_recv.at[tp], (sp, tp_x)),
        remote(ow_in, ow.at[tp], ow_send.at[1], ow_recv.at[tp], (sp, tp_core)),
        remote(ow.at[tp_x], ow.at[tp_x], ow_send.at[2], ow_recv.at[tp_x], (sp, tp_core)),
    ]
    ow_copies[0].start()
    ow_copies[1].start()

    for i in range(3):
        local_copy(i).wait()
    row_index = lax.broadcasted_iota(jnp.int32, (BLOCK, BLOCK), 0)
    col_index = lax.broadcasted_iota(jnp.int32, (BLOCK, BLOCK), 1)
    before = jnp.where(row_index <= col_index, 1.0, 0.0)
    until = jnp.where(row_index >= col_index, 1.0, 0.0)
    for b in range(block_count):
        decay = decay_in[:, b * BLOCK : (b + 1) * BLOCK]
        cum_row[b] = jnp.dot(
            decay, before, preferred_element_type=F32, precision=lax.Precision.HIGHEST
        )
        cum_col[b] = lax.dot_general(
            until,
            decay,
            (((1,), (1,)), ((), ())),
            preferred_element_type=F32,
            precision=lax.Precision.HIGHEST,
        )

    def block_decay(b, h):
        return jnp.exp(cum_row[b, h : h + 1, BLOCK - 1 : BLOCK])

    for h in range(heads):
        lanes = slice(h * dim, (h + 1) * dim)
        for b in range(block_count):
            span = slice(b * BLOCK, (b + 1) * BLOCK)
            last = cum_row[b, h : h + 1, BLOCK - 1 : BLOCK]
            to_end = jnp.exp(last - cum_col[b, :, h : h + 1]) * scale
            scaled = (k_ref[span, lanes].astype(F32) * to_end).astype(BF16)
            local_state[b, h] = lax.dot_general(
                scaled, v_ref[span, lanes], (((0,), (0,)), ((), ())), preferred_element_type=F32
            )

    def local_total(h):
        total, decay = local_state[0, h], block_decay(0, h)
        for b in range(1, block_count):
            total = block_decay(b, h) * total + local_state[b, h]
            decay = decay * block_decay(b, h)
        return total, decay

    header_row = lax.broadcasted_iota(jnp.int32, (HEADER_ROWS, dim), 0)

    def pack(ref, h, total, decay):
        ref[h, :dim] = total.astype(BF16)
        wide = jnp.broadcast_to(decay, (HEADER_ROWS, dim))
        high = wide.astype(BF16).astype(F32)
        ref[h, dim:] = jnp.where(header_row < 8, high, wide - high).astype(BF16)

    def unpack(packed, h):
        block = packed[h].astype(F32)
        return block[:dim], block[dim : dim + 1] + block[dim + 8 : dim + 9]

    for h in range(heads):
        total, decay = local_total(h)
        pack(state_out, h, total, decay)
    pair_copy = remote(state_out, state_pair, pair_send.at[0], pair_recv.at[0], (sp_y, tp))
    pair_copy.start()
    start_own(0)

    def scores_of(b):
        for h in range(heads):
            lanes = slice(h * dim, (h + 1) * dim)
            span = slice(b * BLOCK, (b + 1) * BLOCK)
            tile = 128
            keys, vals = k_ref[span, lanes], v_ref[span, lanes]
            row_sums = cum_row[b, h : h + 1, :]

            def one(i, _):
                at = pl.multiple_of(i * tile, tile)
                here = pl.ds(b * BLOCK + at, tile)
                products = lax.dot_general(
                    q_ref[here, lanes], keys, (((1,), (1,)), ((), ())), preferred_element_type=F32
                )
                gap = cum_col[b, pl.ds(at, tile), h : h + 1] - row_sums
                t_index = at + lax.broadcasted_iota(jnp.int32, (tile, BLOCK), 0)
                s_index = lax.broadcasted_iota(jnp.int32, (tile, BLOCK), 1)
                weight = jnp.where(s_index <= t_index, jnp.exp(jnp.minimum(gap, 0.0)), 0.0)
                scores = (products * scale * weight).astype(BF16)
                retention[here, lanes] = jnp.dot(scores, vals, preferred_element_type=F32)
                return 0

            lax.fori_loop(0, BLOCK // tile, one, 0)

    scores_of(0)

    pair_copy.wait_recv()
    for h in range(heads):
        total, decay = local_total(h)
        their_total, their_decay = unpack(state_pair, h)
        last_factor = jnp.where(y == 1, decay, their_decay)
        first = jnp.where(y == 1, their_total, total)
        second = jnp.where(y == 1, total, their_total)
        pack(total_out, h, last_factor * first + second, decay * their_decay)

    def total_copy(plane):
        return remote(
            total_out,
            total_in.at[z],
            total_send.at[plane],
            total_recv.at[z],
            (plane * 2 + y, tp),
        )

    for plane in range(1, 4):

        @pl.when(z < plane)
        def _():
            total_copy(plane).start()

    start_z(1)
    for b in range(1, block_count):
        scores_of(b)

    ow_arrival = [
        remote(ow.at[t], ow.at[t], ow_send.at[0], ow_recv.at[t], (sp, tp_x))
        for t in (tp_x, tp_core, tp_both)
    ]

    for h in range(heads):
        start_state[0, h] = jnp.zeros((dim, dim), F32)
    for plane in range(3):

        @pl.when(plane < z)
        def _():
            remote(
                total_out,
                total_in.at[plane],
                total_send.at[plane],
                total_recv.at[plane],
                (sp_y, tp),
            ).wait_recv()
            for h in range(heads):
                total, decay = unpack(total_in.at[plane], h)
                start_state[0, h] = decay * start_state[0, h] + total

    for h in range(heads):
        their_total, their_decay = unpack(state_pair, h)
        state = start_state[0, h]
        state = jnp.where(y == 1, their_decay * state + their_total, state)
        start_state[0, h] = state
        for b in range(1, block_count):
            state = block_decay(b - 1, h) * state + local_state[b - 1, h]
            start_state[b, h] = state

    local_copy(3).wait()

    def retained_copy(j):
        return remote(
            retained_out.at[j],
            retained_in.at[tp],
            ret_send.at[j],
            ret_recv.at[tp],
            (sp, j),
        )

    per_block = BLOCK // quarter

    def finish(j, target):
        b = j // per_block
        at = pl.multiple_of((j % per_block) * quarter, quarter)
        here = pl.ds(pl.multiple_of(j * quarter, quarter), quarter)
        for h in range(heads):
            lanes = slice(h * dim, (h + 1) * dim)
            state = start_state[b, h]
            high = state.astype(BF16)
            low = (state - high.astype(F32)).astype(BF16)
            query = q_ref[here, lanes]
            carried = jnp.dot(query, high, preferred_element_type=F32) + jnp.dot(
                query, low, preferred_element_type=F32
            )
            kept = retention[here, lanes] + carried * jnp.exp(
                cum_col[b, pl.ds(at, quarter), h : h + 1]
            )
            centered = kept - jnp.mean(kept, axis=-1, keepdims=True)
            variance = jnp.mean(centered * centered, axis=-1, keepdims=True)
            normed = centered * lax.rsqrt(variance + EPSILON) * norm_gain[h : h + 1, :]
            target[:, lanes] = (silu_of(gates_ref[here, lanes].astype(F32)) * normed).astype(BF16)

    others = [(tp + i) % tps for i in range(1, tps)]
    for j in others:
        finish(j, retained_out.at[j])
        retained_copy(j).start()
    finish(tp, retained_in.at[tp])

    pass_z(0, near_planes[:1])
    ow_arrival[0].wait_recv()
    ow_copies[2].start()
    for arrival in ow_arrival[1:]:
        arrival.wait_recv()
    local_copy(5).wait()
    local_copy(4).wait()
    for j in others:
        remote(
            retained_out.at[j],
            retained_in.at[j],
            ret_send.at[j],
            ret_recv.at[j],
            (sp, j),
        ).wait_recv()

    mix_tile = 512

    def mix(i, _):
        here = pl.ds(pl.multiple_of(i * mix_tile, mix_tile), mix_tile)
        total = jnp.zeros((quarter, mix_tile), F32)
        for g in range(tps):
            part = jnp.dot(retained_in[g], ow[g, :, here], preferred_element_type=F32)
            total = total + part.astype(BF16).astype(F32)
        mixed[:, here] = total.astype(BF16)
        return 0

    lax.fori_loop(0, model // mix_tile, mix, 0)

    def rms_of(v):
        return v * lax.rsqrt(jnp.mean(v * v, axis=-1, keepdims=True) + EPSILON)

    mine = x * 2 + parity
    norm_tile = 32

    def into_rows(i, _):
        here = pl.ds(pl.multiple_of(i * norm_tile, norm_tile), norm_tile)
        value = rms_of(mixed[here, :].astype(F32)) * mix_gain[...]
        value = (resid_ref[here, :].astype(F32) + value).astype(BF16)
        middle[here, :] = value
        rows[mine, here, :] = (rms_of(value.astype(F32)) * pre_gain[...]).astype(BF16)
        return 0

    lax.fori_loop(0, quarter // norm_tile, into_rows, 0)

    from_pair = x * 2 + 1 - parity
    from_x = other_x * 2 + parity
    from_both = other_x * 2 + 1 - parity

    def rows_copy(i, place, device):
        return remote(rows.at[place], rows.at[place], rows_send.at[i], rows_recv.at[place], device)

    rows_copy(0, mine, (sp_pair, tp)).start()
    rows_copy(1, mine, (sp, tp_x)).start()
    start_z(2)
    start_own(1)
    start_own(2)
    pass_z(0, near_planes[1:])
    pass_y(0, all_planes)
    pass_z(1, near_planes)
    rows_copy(0, from_pair, (sp_pair, tp)).wait_recv()
    rows_copy(2, from_pair, (sp, tp_x)).start()
    pass_y(1, all_planes)
    own_wait(0)
    own_wait(1)
    core_wait(0, all_planes)
    core_wait(1, all_planes)

    unit_tile = 128

    def gate_up(first):
        def one(i, _):
            here = pl.ds(pl.multiple_of(i * unit_tile, unit_tile), unit_tile)
            both = jnp.concatenate(
                [
                    wg[:, :, here].reshape(model, unit_tile),
                    wu[:, :, here].reshape(model, unit_tile),
                ],
                axis=1,
            )
            acts = jnp.dot(
                rows[pl.ds(first, 2)].reshape(2 * quarter, model), both, preferred_element_type=F32
            )
            value = silu_of(acts[:, :unit_tile]) * acts[:, unit_tile:]
            hidden[pl.ds(first, 2), :, here] = value.astype(BF16).reshape(2, quarter, unit_tile)
            return 0

        lax.fori_loop(0, units // unit_tile, one, 0)

    gate_up(x * 2)
    pass_z(2, near_planes)
    rows_copy(1, from_x, (sp, tp_x)).wait_recv()
    rows_copy(2, from_both, (sp, tp_x)).wait_recv()
    gate_up(other_x * 2)
    own_wait(2)

    columns = model // 8

    def down(plane, half, first):
        product = jnp.dot(
            hidden[pl.ds(first, 2)].reshape(2 * quarter, units),
            wd[plane * 2 + half],
            preferred_element_type=F32,
        )
        return product.reshape(2, quarter, columns)

    def part_copy(plane):
        return remote(
            part_out.at[plane],
            part_in.at[plane],
            part_send.at[plane],
            part_recv.at[plane],
            (sp, tp_x),
        )

    for plane in all_planes:
        pass_y(2, [plane])
        core_wait(2, [plane])
        for half in range(2):
            part_out[plane, :, :, half * columns : (half + 1) * columns] = down(
                plane, half, other_x * 2
            ).astype(BF16)
        part_copy(plane).start()

    def sum_copy(plane):
        return remote(
            sum_out.at[plane],
            sum_in.at[plane],
            sum_send.at[plane],
            sum_recv.at[plane],
            (sp_pair, tp),
        )

    for plane in all_planes:
        own_parts = [down(plane, half, x * 2) for half in range(2)]
        part_copy(plane).wait_recv()
        for half in range(2):
            lanes = slice(half * columns, (half + 1) * columns)
            mine_part = jnp.where(parity == 0, own_parts[half][0], own_parts[half][1])
            pair_part = jnp.where(parity == 0, own_parts[half][1], own_parts[half][0])
            sum_out[plane, :, lanes] = (
                pair_part.astype(BF16).astype(F32)
                + part_in[plane, 1 - parity, :, lanes].astype(F32)
            ).astype(BF16)
            branch[plane, :, lanes] = (
                mine_part.astype(BF16).astype(F32) + part_in[plane, parity, :, lanes].astype(F32)
            )
        sum_copy(plane).start()

    for plane in all_planes:
        sum_copy(plane).wait_recv()

    def final(i, _):
        here = pl.ds(pl.multiple_of(i * norm_tile, norm_tile), norm_tile)
        value = jnp.concatenate(
            [branch[n, here, :] + sum_in[n, here, :].astype(F32) for n in range(planes)], axis=1
        )
        value = rms_of(value.astype(BF16).astype(F32)) * post_gain[...]
        out[here, :] = (middle[here, :].astype(F32) + value).astype(BF16)
        return 0

    lax.fori_loop(0, quarter // norm_tile, final, 0)

    for m in range(3):
        z_far(m).wait_send()

        @pl.when(is_helper)
        def _():
            z_near(m).wait_send()

        @pl.when(is_main)
        def _():
            for plane in all_planes:
                src = weights_in[m] if plane is z else slot(m, plane * 2 + y)
                to_y(m, plane, src).wait_send()
                to_core(m, plane * 2 + y, src).wait_send()
                place = plane * 2 + other_y
                to_core(m, place, slot(m, place)).wait_send()

    for copy in ow_copies:
        copy.wait_send()
    pair_copy.wait_send()
    for plane in range(1, 4):

        @pl.when(z < plane)
        def _():
            total_copy(plane).wait_send()

    for j in others:
        retained_copy(j).wait_send()
    rows_copy(0, mine, (sp_pair, tp)).wait_send()
    rows_copy(1, mine, (sp, tp_x)).wait_send()
    rows_copy(2, from_pair, (sp, tp_x)).wait_send()
    for plane in range(4):
        part_copy(plane).wait_send()
        sum_copy(plane).wait_send()


def whole_layer(
    queries,
    keys,
    values,
    gates,
    log_decay,
    norm_gain,
    out_weight,
    resid,
    post_mix_gain,
    pre_ffn_gain,
    w_gate,
    w_up,
    w_down,
    post_ffn_gain,
):
    places, tps = lax.axis_size("sp"), lax.axis_size("tp")
    planes = places // 2
    row_count, width = queries.shape
    heads, dim = norm_gain.shape
    block_count = row_count // BLOCK
    quarter, model = resid.shape
    depth, units = w_gate.shape
    columns = w_down.shape[1]
    decay_rows = jnp.pad(log_decay.T, ((0, 8 - heads), (0, 0)))
    anywhere = pl.BlockSpec(memory_space=pl.ANY)
    onchip = pl.BlockSpec(memory_space=pltpu.VMEM)
    dma = pltpu.SemaphoreType.DMA
    packed = (heads, dim + HEADER_ROWS, dim)
    scratch = [
        pltpu.VMEM((row_count, width), BF16),
        pltpu.VMEM((row_count, width), BF16),
        pltpu.VMEM((row_count, width), BF16),
        pltpu.VMEM((row_count, width), BF16),
        pltpu.VMEM((quarter, model), BF16),
        pltpu.VMEM((places, depth, units), BF16),
        pltpu.VMEM((places, depth, units), BF16),
        pltpu.VMEM((places, units, columns), BF16),
        pltpu.VMEM((tps, width, model), BF16),
        pltpu.VMEM((block_count, 8, BLOCK), F32),
        pltpu.VMEM((block_count, BLOCK, 8), F32),
        pltpu.VMEM((block_count, heads, dim, dim), F32),
        pltpu.VMEM((block_count, heads, dim, dim), F32),
        pltpu.VMEM(packed, BF16),
        pltpu.VMEM(packed, BF16),
        pltpu.VMEM(packed, BF16),
        pltpu.VMEM((planes,) + packed, BF16),
        pltpu.VMEM((row_count, width), F32),
        pltpu.VMEM((tps, quarter, width), BF16),
        pltpu.VMEM((tps, quarter, width), BF16),
        pltpu.VMEM((quarter, model), BF16),
        pltpu.VMEM((quarter, model), BF16),
        pltpu.VMEM((4, quarter, model), BF16),
        pltpu.VMEM((4, quarter, units), BF16),
        pltpu.VMEM((planes, 2, quarter, 2 * columns), BF16),
        pltpu.VMEM((planes, 2, quarter, 2 * columns), BF16),
        pltpu.VMEM((planes, quarter, 2 * columns), BF16),
        pltpu.VMEM((planes, quarter, 2 * columns), BF16),
        pltpu.VMEM((planes, quarter, 2 * columns), F32),
        dma((6,)),
        dma((3,)),
        dma((3, 2)),
        dma((3, planes)),
        dma((3, planes)),
        dma((3, planes)),
        dma((3, places)),
        dma((3, places)),
        dma((3,)),
        dma((tps,)),
        dma((1,)),
        dma((1,)),
        dma((planes,)),
        dma((planes,)),
        dma((tps,)),
        dma((tps,)),
        dma((3,)),
        dma((4,)),
        dma((planes,)),
        dma((planes,)),
        dma((planes,)),
        dma((planes,)),
    ]
    return pl.pallas_call(
        layer_kernel,
        out_shape=jax.ShapeDtypeStruct((quarter, model), BF16),
        in_specs=[anywhere] * 4
        + [onchip, onchip, anywhere, anywhere, onchip, onchip]
        + [anywhere] * 3
        + [onchip],
        out_specs=onchip,
        scratch_shapes=scratch,
        compiler_params=pltpu.CompilerParams(
            collective_id=0, has_side_effects=True, vmem_limit_bytes=62 * 1024 * 1024
        ),
    )(
        queries,
        keys,
        values,
        gates,
        decay_rows,
        norm_gain,
        out_weight,
        resid,
        post_mix_gain[None],
        pre_ffn_gain[None],
        w_gate,
        w_up,
        w_down,
        post_ffn_gain[None],
    )


def solution(mesh):
    in_specs = (
        P("sp", "tp"),
        P("sp", "tp"),
        P("sp", "tp"),
        P("sp", "tp"),
        P("sp", "tp"),
        P("tp", None),
        P("tp", None),
        P(("sp", "tp"), None),
        P(),
        P(),
        P("sp", "tp"),
        P("sp", "tp"),
        P("tp", "sp"),
        P(),
    )
    out_specs = P(("sp", "tp"), None)
    if mesh.shape["sp"] == LONGEST_RING and mesh.shape["tp"] == 4:
        return jax.shard_map(
            whole_layer, mesh=mesh, in_specs=in_specs, out_specs=out_specs, check_vma=False
        )

    return jax.shard_map(
        per_device, mesh=mesh, in_specs=in_specs, out_specs=out_specs, check_vma=False
    )
```

profile of v0, /device:TPU:16, one launch (start us, length us, event | category | flops | bytes accessed | tf_op | source)
XLA Modules:
  0.0 199.4 jit_solution(10160233946409924434)
XLA Ops:
  0.0 1.3 pad.4.decay_in
  1.3 195.8 %shard_map.136 = bf16[256,2048]{1,0:T(8,128)(2,1)} custom-call(bf16[1024,256]{1,0:T(8,128)(2,1)} %q_in.1, bf16[1024,256]{1,0:T(8,128)(2,1)} %k_in.1, bf16[1024,256]{1,0:T(8,128)(2,1)} %v_in.1, bf16[1024,256]{1,0:T(8,128)(2,1)} %gates_in.1, f32[8,1024]{1,0:T(8,128)} %pad.4.decay_in, f32[2,128]{1,0:T(2,128)} %norm_gain.1, bf16[256,2048]{1,0:T(8,128)(2,1)} %ow_in.1, ...), custom_call_target="tpu_custom_call" | custom-call | tf_op jit(solution)/shard_map/pallas_call | solution.py:987
  197.1 2.3 %copy.16 = bf16[256,2048]{1,0:T(8,128)(2,1)} copy(bf16[256,2048]{1,0:T(8,128)(2,1)} %shard_map.136) | data formatting | bytes 2097152
where the time goes:
time: 200 us; the launch traced here: 199 us
  Pallas kernels  196 us (98%)
  local copies, waits for them, and re-layouts  3.62 us (2%)
    pallas_call x1, Pallas kernels, whole_layer(): pl.pallas_call(layer_kernel, out_shape=jax.ShapeDtypeStruct((quarter, mod...  196 us

commit v1 on v0

--- a/solution.py
+++ b/solution.py
@@ -325,6 +325,7 @@
     mixed,
     middle,
     rows,
+    gate_acts,
     hidden,
     part_out,
     part_in,
@@ -425,90 +426,136 @@
     pl.semaphore_wait(barrier, len(peers))
 
     far_target = lax.select(is_main, far, far_pair)
-
-    def z_near(m):
+    in_middle = jnp.logical_and(z > 0, z < planes - 1)
+    at_end = jnp.logical_or(z == 0, z == planes - 1)
+
+    def cut(ref, half):
+        size = ref.shape[0] // 2
+        return ref.at[half * size : (half + 1) * size]
+
+    def source(m, half):
+        return cut(weights_in[m], half)
+
+    def slot(m, half, place):
+        size = weights[m].shape[1] // 2
+        return weights[m].at[place, half * size : (half + 1) * size]
+
+    def z_near(m, half):
+        piece = 2 * m + half
         return remote(
-            weights_in[m], weights[m].at[sp], z_send.at[m, 0], z_recv.at[m, z], (pair * 2 + y, tp)
-        )
-
-    def z_far(m):
+            source(m, half),
+            slot(m, half, sp),
+            z_send.at[piece, 0],
+            z_recv.at[piece, z],
+            (pair * 2 + y, tp),
+        )
+
+    def z_far(m, half):
+        piece = 2 * m + half
         return remote(
-            weights_in[m],
-            weights[m].at[sp],
-            z_send.at[m, 1],
-            z_recv.at[m, z],
+            source(m, half),
+            slot(m, half, sp),
+            z_send.at[piece, 1],
+            z_recv.at[piece, z],
             (far_target * 2 + y, tp),
         )
 
-    def start_z(m):
-        @pl.when(is_helper)
-        def _():
-            z_near(m).start()
-
-        z_far(m).start()
-
-    def slot(m, source):
-        return weights[m].at[source]
-
-    def to_y(m, plane, src):
-        place = plane * 2 + y
+    def to_y(m, half, plane, src):
+        piece, place = 2 * m + half, plane * 2 + y
         return remote(
-            src, slot(m, place), y_send.at[m, plane], y_recv.at[m, plane], (sp_y, tp)
-        )
-
-    def to_core(m, place, src):
+            src,
+            slot(m, half, place),
+            y_send.at[piece, plane],
+            y_recv.at[piece, plane],
+            (sp_y, tp),
+        )
+
+    def to_core(m, half, place, src):
+        piece = 2 * m + half
         return remote(
-            src, slot(m, place), c_send.at[m, place], c_recv.at[m, place], (sp, tp_core)
-        )
-
-    def z_arrival(m, plane):
-        place = plane * 2 + y
-        return remote(
-            slot(m, place), slot(m, place), z_send.at[m, 1], z_recv.at[m, plane], (sp_y, tp)
-        )
-
-    def y_arrival(m, plane):
-        place = plane * 2 + other_y
-        return remote(
-            slot(m, place), slot(m, place), y_send.at[m, plane], y_recv.at[m, plane], (sp_y, tp)
-        )
+            src,
+            slot(m, half, place),
+            c_send.at[piece, place],
+            c_recv.at[piece, place],
+            (sp, tp_core),
+        )
+
+    def z_arrival(m, half, plane):
+        piece, here = 2 * m + half, slot(m, half, plane * 2 + y)
+        return remote(here, here, z_send.at[piece, 1], z_recv.at[piece, plane], (sp_y, tp))
+
+    def y_arrival(m, half, plane):
+        piece, here = 2 * m + half, slot(m, half, plane * 2 + other_y)
+        return remote(here, here, y_send.at[piece, plane], y_recv.at[piece, plane], (sp_y, tp))
 
     def start_own(m):
         @pl.when(is_main)
         def _():
-            to_y(m, z, weights_in[m]).start()
-            to_core(m, sp, weights_in[m]).start()
-
-    def pass_z(m, planes_list):
+            for half in range(2):
+                to_y(m, half, z, source(m, half)).start()
+                to_core(m, half, sp, source(m, half)).start()
+
+    def pass_plane(m, half, plane):
+        z_arrival(m, half, plane).wait_recv()
+        here = slot(m, half, plane * 2 + y)
+        to_y(m, half, plane, here).start()
+        to_core(m, half, plane * 2 + y, here).start()
+
+    def pass_z(m, half, planes_list):
         @pl.when(is_main)
         def _():
             for plane in planes_list:
-                z_arrival(m, plane).wait_recv()
-                place = plane * 2 + y
-                to_y(m, plane, slot(m, place)).start()
-                to_core(m, place, slot(m, place)).start()
-
-    def pass_y(m, planes_list):
+                pass_plane(m, half, plane)
+
+    def pass_if(condition, m, half, plane):
+        @pl.when(jnp.logical_and(condition, is_main))
+        def _():
+            pass_plane(m, half, plane)
+
+    def pass_y(m, half, planes_list):
         @pl.when(is_main)
         def _():
             for plane in planes_list:
-                y_arrival(m, plane).wait_recv()
+                y_arrival(m, half, plane).wait_recv()
                 place = plane * 2 + other_y
-                to_core(m, place, slot(m, place)).start()
+                to_core(m, half, place, slot(m, half, place)).start()
 
     def core_wait(m, planes_list):
         @pl.when(is_helper)
         def _():
             for plane in planes_list:
-                for place in (plane * 2 + y, plane * 2 + other_y):
-                    to_core(m, place, slot(m, place)).wait_recv()
+                for half in range(2):
+                    for place in (plane * 2 + y, plane * 2 + other_y):
+                        here = slot(m, half, place)
+                        to_core(m, half, place, here).wait_recv()
 
     def own_wait(m):
         @pl.when(is_main)
         def _():
             own_copy(m).wait()
 
-    start_z(0)
+    near_up = parity == 0
+    far_up = z < planes // 2
+    near_down, far_down = parity == 1, z >= planes // 2
+    one_hop = jnp.logical_and(in_middle, is_helper)
+    more_hops = jnp.logical_or(at_end, is_main)
+    both = jnp.logical_and
+
+    def when_do(condition, do):
+        @pl.when(condition)
+        def _():
+            do()
+
+    def start_far(m, half, condition):
+        when_do(condition, lambda: z_far(m, half).start())
+
+    def start_near(m, half, condition):
+        when_do(both(is_helper, condition), lambda: z_near(m, half).start())
+
+    when_do(is_helper, lambda: z_near(0, 0).start())
+    start_far(0, 0, jnp.logical_or(far_down, one_hop))
+    start_near(0, 1, near_down)
+    start_far(0, 1, far_down)
     near_planes = [pair, far, far_pair]
     all_planes = [z] + near_planes
 
@@ -522,6 +569,7 @@
 
     for i in range(3):
         local_copy(i).wait()
+
     row_index = lax.broadcasted_iota(jnp.int32, (BLOCK, BLOCK), 0)
     col_index = lax.broadcasted_iota(jnp.int32, (BLOCK, BLOCK), 1)
     before = jnp.where(row_index <= col_index, 1.0, 0.0)
@@ -629,7 +677,10 @@
         def _():
             total_copy(plane).start()
 
-    start_z(1)
+
+    for half in range(2):
+        start_far(1, half, both(far_down, in_middle))
+        start_near(1, half, near_down)
     for b in range(1, block_count):
         scores_of(b)
 
@@ -699,12 +750,20 @@
             target[:, lanes] = (silu_of(gates_ref[here, lanes].astype(F32)) * normed).astype(BF16)
 
     others = [(tp + i) % tps for i in range(1, tps)]
+    start_near(0, 1, near_up)
+    start_far(0, 0, both(far_up, more_hops))
+    start_far(0, 1, far_up)
+    for half in range(2):
+        start_far(1, half, both(far_up, in_middle))
+        start_near(1, half, near_up)
+
     for j in others:
         finish(j, retained_out.at[j])
         retained_copy(j).start()
     finish(tp, retained_in.at[tp])
 
-    pass_z(0, near_planes[:1])
+    pass_z(0, 0, near_planes[:1])
+    start_own(1)
     ow_arrival[0].wait_recv()
     ow_copies[2].start()
     for arrival in ow_arrival[1:]:
@@ -747,58 +806,100 @@
         rows[mine, here, :] = (rms_of(value.astype(F32)) * pre_gain[...]).astype(BF16)
         return 0
 
-    lax.fori_loop(0, quarter // norm_tile, into_rows, 0)
-
     from_pair = x * 2 + 1 - parity
     from_x = other_x * 2 + parity
     from_both = other_x * 2 + 1 - parity
-
-    def rows_copy(i, place, device):
-        return remote(rows.at[place], rows.at[place], rows_send.at[i], rows_recv.at[place], device)
-
-    rows_copy(0, mine, (sp_pair, tp)).start()
-    rows_copy(1, mine, (sp, tp_x)).start()
-    start_z(2)
-    start_own(1)
+    half_rows = quarter // 2
+
+    def rows_copy(i, half, place, device):
+        here = rows.at[place, half * half_rows : (half + 1) * half_rows]
+        return remote(here, here, rows_send.at[i, half], rows_recv.at[place, half], device)
+
+    for half in range(2):
+        steps = half_rows // norm_tile
+        lax.fori_loop(half * steps, (half + 1) * steps, into_rows, 0)
+        rows_copy(0, half, mine, (sp_pair, tp)).start()
+        rows_copy(1, half, mine, (sp, tp_x)).start()
+
+    for half in range(2):
+        start_far(2, half, one_hop)
+    pass_z(0, 1, near_planes[:1])
+    pass_z(0, 0, near_planes[1:])
+    pass_z(0, 1, near_planes[1:])
+    for half in range(2):
+        pass_z(1, half, near_planes[:1])
+    rows_copy(0, 0, from_pair, (sp_pair, tp)).wait_recv()
+    rows_copy(2, 0, from_pair, (sp, tp_x)).start()
+    for half in range(2):
+        start_far(1, half, at_end)
     start_own(2)
-    pass_z(0, near_planes[1:])
-    pass_y(0, all_planes)
-    pass_z(1, near_planes)
-    rows_copy(0, from_pair, (sp_pair, tp)).wait_recv()
-    rows_copy(2, from_pair, (sp, tp_x)).start()
-    pass_y(1, all_planes)
+    for half in range(2):
+        pass_if(at_end, 1, half, far)
+        pass_if(in_middle, 1, half, far_pair)
+    rows_copy(0, 1, from_pair, (sp_pair, tp)).wait_recv()
+    rows_copy(2, 1, from_pair, (sp, tp_x)).start()
+    for half in range(2):
+        when_do(is_helper, lambda: z_near(2, half).start())
+        start_far(2, half, more_hops)
+    for half in range(2):
+        pass_y(0, half, all_planes)
     own_wait(0)
+    core_wait(0, all_planes)
+
+    unit_tile = 256
+    unit_steps = units // unit_tile
+
+    def acts_of(weight, first, at, size):
+        here = pl.ds(at, size)
+        return jnp.dot(
+            rows[pl.ds(first, 2)].reshape(2 * quarter, model),
+            weight[:, :, here].reshape(model, size),
+            preferred_element_type=F32,
+        ).reshape(2, quarter, size)
+
+    def over_units(one):
+        def step(i, _):
+            one(pl.multiple_of(i * unit_tile, unit_tile), unit_tile)
+            return 0
+
+        lax.fori_loop(0, unit_steps, step, 0)
+        if units % unit_tile:
+            one(unit_steps * unit_tile, units % unit_tile)
+
+    def gate_of(first):
+        def one(at, size):
+            gate_acts[pl.ds(first, 2), :, pl.ds(at, size)] = acts_of(wg, first, at, size)
+
+        over_units(one)
+
+    def up_of(first):
+        def one(at, size):
+            here = pl.ds(at, size)
+            gate = gate_acts[pl.ds(first, 2), :, here]
+            value = silu_of(gate) * acts_of(wu, first, at, size)
+            hidden[pl.ds(first, 2), :, here] = value.astype(BF16)
+
+        over_units(one)
+
+    gate_of(x * 2)
+    pass_if(at_end, 1, 0, far_pair)
+    pass_if(in_middle, 1, 0, far)
+    pass_if(at_end, 1, 1, far_pair)
+    pass_if(in_middle, 1, 1, far)
+    for half in range(2):
+        rows_copy(1, half, from_x, (sp, tp_x)).wait_recv()
+        rows_copy(2, half, from_both, (sp, tp_x)).wait_recv()
+    gate_of(other_x * 2)
+    pass_z(2, 0, near_planes[:1])
+    pass_y(1, 0, all_planes)
+    for half in range(2):
+        pass_if(in_middle, 2, half, far_pair)
+    pass_y(1, 1, all_planes)
+    pass_if(at_end, 2, 0, far)
+    pass_if(at_end, 2, 0, far_pair)
+    pass_if(in_middle, 2, 0, far)
     own_wait(1)
-    core_wait(0, all_planes)
     core_wait(1, all_planes)
-
-    unit_tile = 128
-
-    def gate_up(first):
-        def one(i, _):
-            here = pl.ds(pl.multiple_of(i * unit_tile, unit_tile), unit_tile)
-            both = jnp.concatenate(
-                [
-                    wg[:, :, here].reshape(model, unit_tile),
-                    wu[:, :, here].reshape(model, unit_tile),
-                ],
-                axis=1,
-            )
-            acts = jnp.dot(
-                rows[pl.ds(first, 2)].reshape(2 * quarter, model), both, preferred_element_type=F32
-            )
-            value = silu_of(acts[:, :unit_tile]) * acts[:, unit_tile:]
-            hidden[pl.ds(first, 2), :, here] = value.astype(BF16).reshape(2, quarter, unit_tile)
-            return 0
-
-        lax.fori_loop(0, units // unit_tile, one, 0)
-
-    gate_up(x * 2)
-    pass_z(2, near_planes)
-    rows_copy(1, from_x, (sp, tp_x)).wait_recv()
-    rows_copy(2, from_both, (sp, tp_x)).wait_recv()
-    gate_up(other_x * 2)
-    own_wait(2)
 
     columns = model // 8
 
@@ -819,14 +920,27 @@
             (sp, tp_x),
         )
 
-    for plane in all_planes:
-        pass_y(2, [plane])
+    def part_of(plane):
+        for half in range(2):
+            pass_y(2, half, [plane])
         core_wait(2, [plane])
         for half in range(2):
             part_out[plane, :, :, half * columns : (half + 1) * columns] = down(
                 plane, half, other_x * 2
             ).astype(BF16)
         part_copy(plane).start()
+
+    up_of(other_x * 2)
+    own_wait(2)
+    part_of(z)
+    pass_z(2, 1, near_planes[:1])
+    pass_if(at_end, 2, 1, far)
+    pass_if(at_end, 2, 1, far_pair)
+    pass_if(in_middle, 2, 1, far)
+    part_of(near_planes[0])
+    up_of(x * 2)
+    for plane in near_planes[1:]:
+        part_of(plane)
 
     def sum_copy(plane):
         return remote(
@@ -868,20 +982,19 @@
     lax.fori_loop(0, quarter // norm_tile, final, 0)
 
     for m in range(3):
-        z_far(m).wait_send()
-
-        @pl.when(is_helper)
-        def _():
-            z_near(m).wait_send()
-
-        @pl.when(is_main)
-        def _():
-            for plane in all_planes:
-                src = weights_in[m] if plane is z else slot(m, plane * 2 + y)
-                to_y(m, plane, src).wait_send()
-                to_core(m, plane * 2 + y, src).wait_send()
-                place = plane * 2 + other_y
-                to_core(m, place, slot(m, place)).wait_send()
+        for half in range(2):
+            z_far(m, half).wait_send()
+            when_do(is_helper, lambda: z_near(m, half).wait_send())
+
+            @pl.when(is_main)
+            def _():
+                for plane in all_planes:
+                    place = plane * 2 + y
+                    src = source(m, half) if plane is z else slot(m, half, place)
+                    to_y(m, half, plane, src).wait_send()
+                    to_core(m, half, place, src).wait_send()
+                    place = plane * 2 + other_y
+                    to_core(m, half, place, slot(m, half, place)).wait_send()
 
     for copy in ow_copies:
         copy.wait_send()
@@ -894,9 +1007,10 @@
 
     for j in others:
         retained_copy(j).wait_send()
-    rows_copy(0, mine, (sp_pair, tp)).wait_send()
-    rows_copy(1, mine, (sp, tp_x)).wait_send()
-    rows_copy(2, from_pair, (sp, tp_x)).wait_send()
+    for half in range(2):
+        rows_copy(0, half, mine, (sp_pair, tp)).wait_send()
+        rows_copy(1, half, mine, (sp, tp_x)).wait_send()
+        rows_copy(2, half, from_pair, (sp, tp_x)).wait_send()
     for plane in range(4):
         part_copy(plane).wait_send()
         sum_copy(plane).wait_send()
@@ -955,6 +1069,7 @@
         pltpu.VMEM((quarter, model), BF16),
         pltpu.VMEM((quarter, model), BF16),
         pltpu.VMEM((4, quarter, model), BF16),
+        pltpu.VMEM((4, quarter, units), F32),
         pltpu.VMEM((4, quarter, units), BF16),
         pltpu.VMEM((planes, 2, quarter, 2 * columns), BF16),
         pltpu.VMEM((planes, 2, quarter, 2 * columns), BF16),
@@ -963,12 +1078,12 @@
         pltpu.VMEM((planes, quarter, 2 * columns), F32),
         dma((6,)),
         dma((3,)),
-        dma((3, 2)),
-        dma((3, planes)),
-        dma((3, planes)),
-        dma((3, planes)),
-        dma((3, places)),
-        dma((3, places)),
+        dma((6, 2)),
+        dma((6, planes)),
+        dma((6, planes)),
+        dma((6, planes)),
+        dma((6, places)),
+        dma((6, places)),
         dma((3,)),
         dma((tps,)),
         dma((1,)),
@@ -977,8 +1092,8 @@
         dma((planes,)),
         dma((tps,)),
         dma((tps,)),
-        dma((3,)),
-        dma((4,)),
+        dma((3, 2)),
+        dma((4, 2)),
         dma((planes,)),
         dma((planes,)),
         dma((planes,)),

time: 200 us -> 167 us (0.83)
  Pallas kernels: 196 us -> 162 us
    pallas_call x1, Pallas kernels: 196 us -> 162 us  [whole_layer(): pl.pallas_call(layer_kernel, out_shape=jax.ShapeDtypeStruct((quarter, mod...]
where the time goes in v1:
time: 167 us; the launch traced here: 166 us
  Pallas kernels  162 us (97%)
  local copies, waits for them, and re-layouts  3.62 us (2%)
    pallas_call x1, Pallas kernels, whole_layer(): pl.pallas_call(layer_kernel, out_shape=jax.ShapeDtypeStruct((quarter, mod...  162 us

profile of v1, /device:TPU:16, one launch (start us, length us, event | category | flops | bytes accessed | tf_op | source)
XLA Modules:
  0.0 166.0 jit_solution(6927850607987473023)
XLA Ops:
  0.0 1.3 pad.4.decay_in
  1.3 162.4 %shard_map.136 = bf16[256,2048]{1,0:T(8,128)(2,1)} custom-call(bf16[1024,256]{1,0:T(8,128)(2,1)} %q_in.1, bf16[1024,256]{1,0:T(8,128)(2,1)} %k_in.1, bf16[1024,256]{1,0:T(8,128)(2,1)} %v_in.1, bf16[1024,256]{1,0:T(8,128)(2,1)} %gates_in.1, f32[8,1024]{1,0:T(8,128)} %pad.4.decay_in, f32[2,128]{1,0:T(2,128)} %norm_gain.1, bf16[256,2048]{1,0:T(8,128)(2,1)} %ow_in.1, ...), custom_call_target="tpu_custom_call" | custom-call | tf_op jit(solution)/shard_map/pallas_call | solution.py:1102
  163.7 2.3 %copy.16 = bf16[256,2048]{1,0:T(8,128)(2,1)} copy(bf16[256,2048]{1,0:T(8,128)(2,1)} %shard_map.136) | data formatting | bytes 2097152

commit v2 on v1

--- a/solution.py
+++ b/solution.py
@@ -512,8 +512,8 @@
         def _():
             pass_plane(m, half, plane)
 
-    def pass_y(m, half, planes_list):
-        @pl.when(is_main)
+    def pass_y(m, half, planes_list, condition=True):
+        @pl.when(jnp.logical_and(condition, is_main))
         def _():
             for plane in planes_list:
                 y_arrival(m, half, plane).wait_recv()
@@ -554,7 +554,7 @@
 
     when_do(is_helper, lambda: z_near(0, 0).start())
     start_far(0, 0, jnp.logical_or(far_down, one_hop))
-    start_near(0, 1, near_down)
+    when_do(is_helper, lambda: z_near(0, 1).start())
     start_far(0, 1, far_down)
     near_planes = [pair, far, far_pair]
     all_planes = [z] + near_planes
@@ -572,20 +572,22 @@
 
     row_index = lax.broadcasted_iota(jnp.int32, (BLOCK, BLOCK), 0)
     col_index = lax.broadcasted_iota(jnp.int32, (BLOCK, BLOCK), 1)
-    before = jnp.where(row_index <= col_index, 1.0, 0.0)
-    until = jnp.where(row_index >= col_index, 1.0, 0.0)
+    before = jnp.where(row_index <= col_index, 1.0, 0.0).astype(BF16)
+    until = jnp.where(row_index >= col_index, 1.0, 0.0).astype(BF16)
     for b in range(block_count):
         decay = decay_in[:, b * BLOCK : (b + 1) * BLOCK]
-        cum_row[b] = jnp.dot(
-            decay, before, preferred_element_type=F32, precision=lax.Precision.HIGHEST
-        )
-        cum_col[b] = lax.dot_general(
-            until,
-            decay,
-            (((1,), (1,)), ((), ())),
-            preferred_element_type=F32,
-            precision=lax.Precision.HIGHEST,
-        )
+        high = decay.astype(BF16)
+        rest = decay - high.astype(F32)
+        middle_term = rest.astype(BF16)
+        low = (rest - middle_term.astype(F32)).astype(BF16)
+        by_row, by_col = 0.0, 0.0
+        for term in (low, middle_term, high):
+            by_row = by_row + jnp.dot(term, before, preferred_element_type=F32)
+            by_col = by_col + lax.dot_general(
+                until, term, (((1,), (1,)), ((), ())), preferred_element_type=F32
+            )
+        cum_row[b] = by_row
+        cum_col[b] = by_col
 
     def block_decay(b, h):
         return jnp.exp(cum_row[b, h : h + 1, BLOCK - 1 : BLOCK])
@@ -750,7 +752,6 @@
             target[:, lanes] = (silu_of(gates_ref[here, lanes].astype(F32)) * normed).astype(BF16)
 
     others = [(tp + i) % tps for i in range(1, tps)]
-    start_near(0, 1, near_up)
     start_far(0, 0, both(far_up, more_hops))
     start_far(0, 1, far_up)
     for half in range(2):
@@ -809,38 +810,39 @@
     from_pair = x * 2 + 1 - parity
     from_x = other_x * 2 + parity
     from_both = other_x * 2 + 1 - parity
-    half_rows = quarter // 2
+    row_parts = 4
+    part_rows = quarter // row_parts
 
     def rows_copy(i, half, place, device):
-        here = rows.at[place, half * half_rows : (half + 1) * half_rows]
+        here = rows.at[place, half * part_rows : (half + 1) * part_rows]
         return remote(here, here, rows_send.at[i, half], rows_recv.at[place, half], device)
 
-    for half in range(2):
-        steps = half_rows // norm_tile
+    for half in range(row_parts):
+        steps = part_rows // norm_tile
         lax.fori_loop(half * steps, (half + 1) * steps, into_rows, 0)
         rows_copy(0, half, mine, (sp_pair, tp)).start()
         rows_copy(1, half, mine, (sp, tp_x)).start()
 
-    for half in range(2):
-        start_far(2, half, one_hop)
     pass_z(0, 1, near_planes[:1])
     pass_z(0, 0, near_planes[1:])
     pass_z(0, 1, near_planes[1:])
     for half in range(2):
         pass_z(1, half, near_planes[:1])
-    rows_copy(0, 0, from_pair, (sp_pair, tp)).wait_recv()
-    rows_copy(2, 0, from_pair, (sp, tp_x)).start()
+    for half in range(row_parts // 2):
+        rows_copy(0, half, from_pair, (sp_pair, tp)).wait_recv()
+        rows_copy(2, half, from_pair, (sp, tp_x)).start()
     for half in range(2):
         start_far(1, half, at_end)
     start_own(2)
     for half in range(2):
         pass_if(at_end, 1, half, far)
         pass_if(in_middle, 1, half, far_pair)
-    rows_copy(0, 1, from_pair, (sp_pair, tp)).wait_recv()
-    rows_copy(2, 1, from_pair, (sp, tp_x)).start()
+    for half in range(row_parts // 2, row_parts):
+        rows_copy(0, half, from_pair, (sp_pair, tp)).wait_recv()
+        rows_copy(2, half, from_pair, (sp, tp_x)).start()
     for half in range(2):
         when_do(is_helper, lambda: z_near(2, half).start())
-        start_far(2, half, more_hops)
+        start_far(2, half, in_middle)
     for half in range(2):
         pass_y(0, half, all_planes)
     own_wait(0)
@@ -857,13 +859,13 @@
             preferred_element_type=F32,
         ).reshape(2, quarter, size)
 
-    def over_units(one):
+    def over_units(one, begin=0, end=unit_steps + 1):
         def step(i, _):
             one(pl.multiple_of(i * unit_tile, unit_tile), unit_tile)
             return 0
 
-        lax.fori_loop(0, unit_steps, step, 0)
-        if units % unit_tile:
+        lax.fori_loop(begin, min(end, unit_steps), step, 0)
+        if end > unit_steps and units % unit_tile:
             one(unit_steps * unit_tile, units % unit_tile)
 
     def gate_of(first):
@@ -872,108 +874,136 @@
 
         over_units(one)
 
-    def up_of(first):
+    def up_of(first, begin=0, end=unit_steps + 1):
         def one(at, size):
             here = pl.ds(at, size)
             gate = gate_acts[pl.ds(first, 2), :, here]
             value = silu_of(gate) * acts_of(wu, first, at, size)
             hidden[pl.ds(first, 2), :, here] = value.astype(BF16)
 
-        over_units(one)
+        over_units(one, begin, end)
 
     gate_of(x * 2)
+    for half in range(2):
+        start_far(2, half, at_end)
     pass_if(at_end, 1, 0, far_pair)
     pass_if(in_middle, 1, 0, far)
     pass_if(at_end, 1, 1, far_pair)
     pass_if(in_middle, 1, 1, far)
     for half in range(2):
+        pass_y(1, half, [z, pair])
+        pass_y(1, half, [far], at_end)
+        pass_y(1, half, [far_pair], in_middle)
+    pass_z(2, 0, near_planes[:1])
+    for half in range(row_parts):
         rows_copy(1, half, from_x, (sp, tp_x)).wait_recv()
         rows_copy(2, half, from_both, (sp, tp_x)).wait_recv()
     gate_of(other_x * 2)
-    pass_z(2, 0, near_planes[:1])
-    pass_y(1, 0, all_planes)
     for half in range(2):
-        pass_if(in_middle, 2, half, far_pair)
-    pass_y(1, 1, all_planes)
-    pass_if(at_end, 2, 0, far)
-    pass_if(at_end, 2, 0, far_pair)
-    pass_if(in_middle, 2, 0, far)
+        pass_y(1, half, [far_pair], at_end)
+        pass_y(1, half, [far], in_middle)
+    for half in range(2):
+        pass_y(2, half, [z])
+    pass_z(2, 1, near_planes[:1])
     own_wait(1)
     core_wait(1, all_planes)
 
-    columns = model // 8
-
-    def down(plane, half, first):
-        product = jnp.dot(
-            hidden[pl.ds(first, 2)].reshape(2 * quarter, units),
-            wd[plane * 2 + half],
-            preferred_element_type=F32,
-        )
-        return product.reshape(2, quarter, columns)
-
-    def part_copy(plane):
+    columns = wd_in.shape[1]
+
+    def down(place, first, second):
+        left = jnp.concatenate([hidden[first], hidden[second]], axis=0)
+        product = jnp.dot(left, wd[place], preferred_element_type=F32)
+        return product.astype(BF16).reshape(2, quarter, columns)
+
+    def part_copy(place, over_x):
+        device = (sp, tp_x) if over_x else (sp_pair, tp)
         return remote(
-            part_out.at[plane],
-            part_in.at[plane],
-            part_send.at[plane],
-            part_recv.at[plane],
-            (sp, tp_x),
-        )
-
-    def part_of(plane):
-        for half in range(2):
-            pass_y(2, half, [plane])
-        core_wait(2, [plane])
-        for half in range(2):
-            part_out[plane, :, :, half * columns : (half + 1) * columns] = down(
-                plane, half, other_x * 2
-            ).astype(BF16)
-        part_copy(plane).start()
+            part_out.at[place], part_in.at[place], part_send.at[place], part_recv.at[place], device
+        )
+
+    def sum_copy(place, over_x):
+        device = (sp_pair, tp) if over_x else (sp, tp_x)
+        return remote(
+            sum_out.at[place], sum_in.at[place], sum_send.at[place], sum_recv.at[place], device
+        )
+
+    def place_wait(place):
+        @pl.when(is_helper)
+        def _():
+            for half in range(2):
+                to_core(2, half, place, slot(2, half, place)).wait_recv()
+
+    def send_part(plane, over_x):
+        place = plane * 2 + (y if over_x else other_y)
+        if not over_x and plane is not z:
+            for half in range(2):
+                pass_y(2, half, [plane])
+        place_wait(place)
+        if over_x:
+            part_out[place] = down(place, other_x * 2, other_x * 2 + 1)
+        else:
+            part_out[place] = down(place, 1 - parity, 3 - parity)
+        part_copy(place, over_x).start()
+
+    def own_product(plane):
+        for over_x in (True, False):
+            place = plane * 2 + (y if over_x else other_y)
+            product = down(place, mine, from_pair if over_x else from_x)
+            branch[place] = product[0].astype(F32)
+            sum_out[place] = product[1]
+
+    def own_part(plane, over_x):
+        place = plane * 2 + (y if over_x else other_y)
+        mine_at, other_at = (parity, 1 - parity) if over_x else (x, other_x)
+        part_copy(place, over_x).wait_recv()
+        sum_out[place] = (
+            sum_out[place].astype(F32) + part_in[place, other_at].astype(F32)
+        ).astype(BF16)
+        sum_copy(place, over_x).start()
+        branch[place] = branch[place] + part_in[place, mine_at].astype(F32)
+
+    def pass_late(half):
+        pass_if(at_end, 2, half, far)
+        pass_if(at_end, 2, half, far_pair)
+        pass_if(in_middle, 2, half, far_pair)
+        pass_if(in_middle, 2, half, far)
 
     up_of(other_x * 2)
     own_wait(2)
-    part_of(z)
-    pass_z(2, 1, near_planes[:1])
-    pass_if(at_end, 2, 1, far)
-    pass_if(at_end, 2, 1, far_pair)
-    pass_if(in_middle, 2, 1, far)
-    part_of(near_planes[0])
-    up_of(x * 2)
-    for plane in near_planes[1:]:
-        part_of(plane)
-
-    def sum_copy(plane):
-        return remote(
-            sum_out.at[plane],
-            sum_in.at[plane],
-            sum_send.at[plane],
-            sum_recv.at[plane],
-            (sp_pair, tp),
-        )
+    send_part(z, True)
+    up_of(x * 2, 0, unit_steps // 2)
+    pass_late(0)
+    up_of(x * 2, unit_steps // 2)
+    send_part(z, False)
+    pass_late(1)
+    send_part(pair, True)
+    own_product(z)
+    own_part(z, True)
+    send_part(pair, False)
+    send_part(far, True)
+    own_product(pair)
+    own_part(pair, False)
+    send_part(far, False)
+    send_part(far_pair, True)
+    own_part(pair, True)
+    send_part(far_pair, False)
+    own_product(far)
+    own_product(far_pair)
+    own_part(z, False)
+    own_part(far, True)
+    own_part(far_pair, False)
+    own_part(far_pair, True)
+    own_part(far, False)
 
     for plane in all_planes:
-        own_parts = [down(plane, half, x * 2) for half in range(2)]
-        part_copy(plane).wait_recv()
-        for half in range(2):
-            lanes = slice(half * columns, (half + 1) * columns)
-            mine_part = jnp.where(parity == 0, own_parts[half][0], own_parts[half][1])
-            pair_part = jnp.where(parity == 0, own_parts[half][1], own_parts[half][0])
-            sum_out[plane, :, lanes] = (
-                pair_part.astype(BF16).astype(F32)
-                + part_in[plane, 1 - parity, :, lanes].astype(F32)
-            ).astype(BF16)
-            branch[plane, :, lanes] = (
-                mine_part.astype(BF16).astype(F32) + part_in[plane, parity, :, lanes].astype(F32)
-            )
-        sum_copy(plane).start()
-
-    for plane in all_planes:
-        sum_copy(plane).wait_recv()
+        sum_copy(plane * 2 + y, True).wait_recv()
+        sum_copy(plane * 2 + other_y, False).wait_recv()
 
     def final(i, _):
         here = pl.ds(pl.multiple_of(i * norm_tile, norm_tile), norm_tile)
         value = jnp.concatenate(
-            [branch[n, here, :] + sum_in[n, here, :].astype(F32) for n in range(planes)], axis=1
+            [branch[n, here, :] + sum_in[n, here, :].astype(F32) for n in range(2 * planes)],
+            axis=1,
         )
         value = rms_of(value.astype(BF16).astype(F32)) * post_gain[...]
         out[here, :] = (middle[here, :].astype(F32) + value).astype(BF16)
@@ -1007,13 +1037,15 @@
 
     for j in others:
         retained_copy(j).wait_send()
-    for half in range(2):
+    for half in range(row_parts):
         rows_copy(0, half, mine, (sp_pair, tp)).wait_send()
         rows_copy(1, half, mine, (sp, tp_x)).wait_send()
         rows_copy(2, half, from_pair, (sp, tp_x)).wait_send()
-    for plane in range(4):
-        part_copy(plane).wait_send()
-        sum_copy(plane).wait_send()
+    for plane in range(planes):
+        for over_x in (True, False):
+            place = plane * 2 + (y if over_x else other_y)
+            part_copy(place, over_x).wait_send()
+            sum_copy(place, over_x).wait_send()
 
 
 def whole_layer(
@@ -1040,7 +1072,7 @@
     quarter, model = resid.shape
     depth, units = w_gate.shape
     columns = w_down.shape[1]
-    decay_rows = jnp.pad(log_decay.T, ((0, 8 - heads), (0, 0)))
+    decay_rows = log_decay.T
     anywhere = pl.BlockSpec(memory_space=pl.ANY)
     onchip = pl.BlockSpec(memory_space=pltpu.VMEM)
     dma = pltpu.SemaphoreType.DMA
@@ -1055,8 +1087,8 @@
         pltpu.VMEM((places, depth, units), BF16),
         pltpu.VMEM((places, units, columns), BF16),
         pltpu.VMEM((tps, width, model), BF16),
-        pltpu.VMEM((block_count, 8, BLOCK), F32),
-        pltpu.VMEM((block_count, BLOCK, 8), F32),
+        pltpu.VMEM((block_count, heads, BLOCK), F32),
+        pltpu.VMEM((block_count, BLOCK, heads), F32),
         pltpu.VMEM((block_count, heads, dim, dim), F32),
         pltpu.VMEM((block_count, heads, dim, dim), F32),
         pltpu.VMEM(packed, BF16),
@@ -1071,11 +1103,11 @@
         pltpu.VMEM((4, quarter, model), BF16),
         pltpu.VMEM((4, quarter, units), F32),
         pltpu.VMEM((4, quarter, units), BF16),
-        pltpu.VMEM((planes, 2, quarter, 2 * columns), BF16),
-        pltpu.VMEM((planes, 2, quarter, 2 * columns), BF16),
-        pltpu.VMEM((planes, quarter, 2 * columns), BF16),
-        pltpu.VMEM((planes, quarter, 2 * columns), BF16),
-        pltpu.VMEM((planes, quarter, 2 * columns), F32),
+        pltpu.VMEM((places, 2, quarter, columns), BF16),
+        pltpu.VMEM((places, 2, quarter, columns), BF16),
+        pltpu.VMEM((places, quarter, columns), BF16),
+        pltpu.VMEM((places, quarter, columns), BF16),
+        pltpu.VMEM((places, quarter, columns), F32),
         dma((6,)),
         dma((3,)),
         dma((6, 2)),
@@ -1092,12 +1124,12 @@
         dma((planes,)),
         dma((tps,)),
         dma((tps,)),
-        dma((3, 2)),
-        dma((4, 2)),
-        dma((planes,)),
-        dma((planes,)),
-        dma((planes,)),
-        dma((planes,)),
+        dma((3, 4)),
+        dma((4, 4)),
+        dma((places,)),
+        dma((places,)),
+        dma((places,)),
+        dma((places,)),
     ]
     return pl.pallas_call(
         layer_kernel,

time: 167 us -> 152 us (0.910)
  Pallas kernels: 162 us -> 150 us
    pallas_call x1, Pallas kernels: 162 us -> 150 us  [whole_layer(): pl.pallas_call(layer_kernel, out_shape=jax.ShapeDtypeStruct((quarter, mod...]
where the time goes in v2:
time: 152 us
  Pallas kernels  150 us (99%)
  local copies, waits for them, and re-layouts  2.3 us (2%)
    pallas_call x1, Pallas kernels, whole_layer(): pl.pallas_call(layer_kernel, out_shape=jax.ShapeDtypeStruct((quarter, mod...  150 us

profile of v2, /device:TPU:16, one launch (start us, length us, event | category | flops | bytes accessed | tf_op | source)
XLA Modules:
  0.0 152.2 jit_solution(4783974668553620528)
XLA Ops:
  0.0 149.9 %shard_map.136 = bf16[256,2048]{1,0:T(8,128)(2,1)} custom-call(bf16[1024,256]{1,0:T(8,128)(2,1)} %q_in.1, bf16[1024,256]{1,0:T(8,128)(2,1)} %k_in.1, bf16[1024,256]{1,0:T(8,128)(2,1)} %v_in.1, bf16[1024,256]{1,0:T(8,128)(2,1)} %gates_in.1, f32[2,1024]{1,0:T(2,128)} %bitcast.4, f32[2,128]{1,0:T(2,128)} %norm_gain.1, bf16[256,2048]{1,0:T(8,128)(2,1)} %ow_in.1, ...), custom_call_target="tpu_custom_call" | custom-call | tf_op jit(solution)/shard_map/pallas_call | solution.py:1134
  149.9 2.3 %copy.16 = bf16[256,2048]{1,0:T(8,128)(2,1)} copy(bf16[256,2048]{1,0:T(8,128)(2,1)} %shard_map.136) | data formatting | bytes 2097152

commit v3 on v2

--- a/solution.py
+++ b/solution.py
@@ -915,8 +915,19 @@
         product = jnp.dot(left, wd[place], preferred_element_type=F32)
         return product.astype(BF16).reshape(2, quarter, columns)
 
+    def place_of(plane, over_x):
+        even = plane % 2 == 0
+        return plane * 2 + (lax.select(even, y, other_y) if over_x else lax.select(even, other_y, y))
+
+    def block_of(plane, own):
+        place = plane * 2 + (y if own else other_y)
+        return place, (plane % 2 == 0) if own else (plane % 2 == 1)
+
     def part_copy(place, over_x):
-        device = (sp, tp_x) if over_x else (sp_pair, tp)
+        if isinstance(over_x, bool):
+            device = (sp, tp_x) if over_x else (sp_pair, tp)
+        else:
+            device = (lax.select(over_x, sp, sp_pair), lax.select(over_x, tp_x, tp))
         return remote(
             part_out.at[place], part_in.at[place], part_send.at[place], part_recv.at[place], device
         )
@@ -933,27 +944,27 @@
             for half in range(2):
                 to_core(2, half, place, slot(2, half, place)).wait_recv()
 
-    def send_part(plane, over_x):
-        place = plane * 2 + (y if over_x else other_y)
-        if not over_x and plane is not z:
+    def send_part(plane, own):
+        place, over_x = block_of(plane, own)
+        if not own and plane is not z:
             for half in range(2):
                 pass_y(2, half, [plane])
         place_wait(place)
-        if over_x:
-            part_out[place] = down(place, other_x * 2, other_x * 2 + 1)
-        else:
-            part_out[place] = down(place, 1 - parity, 3 - parity)
+        part_out[place] = down(
+            place,
+            lax.select(over_x, other_x * 2, 1 - parity),
+            lax.select(over_x, other_x * 2 + 1, 3 - parity),
+        )
         part_copy(place, over_x).start()
 
-    def own_product(plane):
-        for over_x in (True, False):
-            place = plane * 2 + (y if over_x else other_y)
-            product = down(place, mine, from_pair if over_x else from_x)
-            branch[place] = product[0].astype(F32)
-            sum_out[place] = product[1]
+    def own_product(plane, over_x):
+        place = place_of(plane, over_x)
+        product = down(place, mine, from_pair if over_x else from_x)
+        branch[place] = product[0].astype(F32)
+        sum_out[place] = product[1]
 
     def own_part(plane, over_x):
-        place = plane * 2 + (y if over_x else other_y)
+        place = place_of(plane, over_x)
         mine_at, other_at = (parity, 1 - parity) if over_x else (x, other_x)
         part_copy(place, over_x).wait_recv()
         sum_out[place] = (
@@ -970,34 +981,40 @@
 
     up_of(other_x * 2)
     own_wait(2)
-    send_part(z, True)
+    when_do(parity == 0, lambda: send_part(z, True))
+    when_do(parity == 1, lambda: send_part(z, False))
     up_of(x * 2, 0, unit_steps // 2)
     pass_late(0)
     up_of(x * 2, unit_steps // 2)
-    send_part(z, False)
+    when_do(parity == 0, lambda: send_part(z, False))
+    when_do(parity == 1, lambda: send_part(z, True))
     pass_late(1)
     send_part(pair, True)
-    own_product(z)
+    own_product(z, True)
+    own_product(z, False)
     own_part(z, True)
     send_part(pair, False)
     send_part(far, True)
-    own_product(pair)
+    own_product(pair, True)
+    own_product(pair, False)
     own_part(pair, False)
     send_part(far, False)
     send_part(far_pair, True)
+    send_part(far_pair, False)
+    own_part(z, False)
     own_part(pair, True)
-    send_part(far_pair, False)
-    own_product(far)
-    own_product(far_pair)
-    own_part(z, False)
+    own_product(far, True)
     own_part(far, True)
+    own_product(far_pair, False)
     own_part(far_pair, False)
+    own_product(far_pair, True)
     own_part(far_pair, True)
+    own_product(far, False)
     own_part(far, False)
 
     for plane in all_planes:
-        sum_copy(plane * 2 + y, True).wait_recv()
-        sum_copy(plane * 2 + other_y, False).wait_recv()
+        for over_x in (True, False):
+            sum_copy(place_of(plane, over_x), over_x).wait_recv()
 
     def final(i, _):
         here = pl.ds(pl.multiple_of(i * norm_tile, norm_tile), norm_tile)
@@ -1043,7 +1060,7 @@
         rows_copy(2, half, from_pair, (sp, tp_x)).wait_send()
     for plane in range(planes):
         for over_x in (True, False):
-            place = plane * 2 + (y if over_x else other_y)
+            place = plane * 2 + int(over_x)
             part_copy(place, over_x).wait_send()
             sum_copy(place, over_x).wait_send()
 

time: 152 us -> 151 us (level); the launches traced: 152 us -> 149 us
  Pallas kernels: 150 us -> 147 us
    pallas_call x1, Pallas kernels: 150 us -> 147 us  [whole_layer(): pl.pallas_call(layer_kernel, out_shape=jax.ShapeDtypeStruct((quarter, mod...]
where the time goes in v3:
time: 151 us; the launch traced here: 149 us
  Pallas kernels  147 us (97%)
  local copies, waits for them, and re-layouts  2.3 us (2%)
    pallas_call x1, Pallas kernels, whole_layer(): pl.pallas_call(layer_kernel, out_shape=jax.ShapeDtypeStruct((quarter, mod...  147 us

profile of v3, /device:TPU:16, one launch (start us, length us, event | category | flops | bytes accessed | tf_op | source)
XLA Modules:
  0.0 149.3 jit_solution(17672654109425872978)
XLA Ops:
  0.0 147.0 %shard_map.136 = bf16[256,2048]{1,0:T(8,128)(2,1)} custom-call(bf16[1024,256]{1,0:T(8,128)(2,1)} %q_in.1, bf16[1024,256]{1,0:T(8,128)(2,1)} %k_in.1, bf16[1024,256]{1,0:T(8,128)(2,1)} %v_in.1, bf16[1024,256]{1,0:T(8,128)(2,1)} %gates_in.1, f32[2,1024]{1,0:T(2,128)} %bitcast.4, f32[2,128]{1,0:T(2,128)} %norm_gain.1, bf16[256,2048]{1,0:T(8,128)(2,1)} %ow_in.1, ...), custom_call_target="tpu_custom_call" | custom-call | tf_op jit(solution)/shard_map/pallas_call | solution.py:1151
  147.0 2.3 %copy.16 = bf16[256,2048]{1,0:T(8,128)(2,1)} copy(bf16[256,2048]{1,0:T(8,128)(2,1)} %shard_map.136) | data formatting | bytes 2097152

commit v4 on v3

--- a/solution.py
+++ b/solution.py
@@ -828,11 +828,14 @@
     pass_z(0, 1, near_planes[1:])
     for half in range(2):
         pass_z(1, half, near_planes[:1])
+    early_far = both(at_end, both(is_main, far_down))
+    for half in range(2):
+        start_far(1, half, early_far)
     for half in range(row_parts // 2):
         rows_copy(0, half, from_pair, (sp_pair, tp)).wait_recv()
         rows_copy(2, half, from_pair, (sp, tp_x)).start()
     for half in range(2):
-        start_far(1, half, at_end)
+        start_far(1, half, both(at_end, jnp.logical_not(early_far)))
     start_own(2)
     for half in range(2):
         pass_if(at_end, 1, half, far)

time: 151 us -> 152 us (level)
  the two profiles are of different devices: /device:TPU:16 before, /device:TPU:5 now
where the time goes in v4:
time: 152 us
  Pallas kernels  150 us (99%)
  local copies, waits for them, and re-layouts  2.3 us (2%)
    pallas_call x1, Pallas kernels, whole_layer(): pl.pallas_call(layer_kernel, out_shape=jax.ShapeDtypeStruct((quarter, mod...  150 us

profile of v4, /device:TPU:5, one launch (start us, length us, event | category | flops | bytes accessed | tf_op | source)
XLA Modules:
  0.0 151.9 jit_solution(6400490795804422753)
XLA Ops:
  0.0 149.6 %shard_map.136 = bf16[256,2048]{1,0:T(8,128)(2,1)} custom-call(bf16[1024,256]{1,0:T(8,128)(2,1)} %q_in.1, bf16[1024,256]{1,0:T(8,128)(2,1)} %k_in.1, bf16[1024,256]{1,0:T(8,128)(2,1)} %v_in.1, bf16[1024,256]{1,0:T(8,128)(2,1)} %gates_in.1, f32[2,1024]{1,0:T(2,128)} %bitcast.4, f32[2,128]{1,0:T(2,128)} %norm_gain.1, bf16[256,2048]{1,0:T(8,128)(2,1)} %ow_in.1, ...), custom_call_target="tpu_custom_call" | custom-call | tf_op jit(solution)/shard_map/pallas_call | solution.py:1154
  149.6 2.3 %copy.16 = bf16[256,2048]{1,0:T(8,128)(2,1)} copy(bf16[256,2048]{1,0:T(8,128)(2,1)} %shard_map.136) | data formatting | bytes 2097152
